TPU v7x, 32 devices: a whole 2x2x4 slice. The times are simulated.
32 devices in a mesh: grp: 2 (over y), dp: 2 (over x), kv: 4 (over z), tp: 2 (over core).
Axes of the slice: x: 2, y: 2, z: 4, core: 2. Of those that a mesh axis runs over, the one named last changes fastest.
Arguments:
- residual_input: bfloat16 [128, 4096], P(('grp', 'dp', 'tp'), 'kv'), parts along dimension 0, may hold values from -6 to 6
- incoming_state: float32 [128, 16, 64, 128], P(('grp', 'kv'), ('dp', 'tp')), parts along dimension 0, may hold values from -4 to 4
- extra_log_decay: float32 [128, 1024], P(('grp', 'kv'), ('dp', 'tp')), parts along dimension 0, may hold values from -0.7 to 0
- leading_norm_gain: float32 [4096], P('kv'), may hold values from 0.1 to 1.9
- leading_gate_weight: bfloat16 [4096, 11264], P('kv', ('dp', 'tp')), may hold values from -0.09375 to 0.09375
- leading_up_weight: bfloat16 [4096, 11264], P('kv', ('dp', 'tp')), may hold values from -0.09375 to 0.09375
- leading_down_weight: bfloat16 [11264, 4096], P(('dp', 'tp'), 'kv'), may hold values from -0.0546875 to 0.0546875
- attention_norm_gain: float32 [4096], P('kv'), may hold values from 0.1 to 1.9
- query_projector: bfloat16 [4096, 1024], P('kv', ('dp', 'tp')), may hold values from -0.09375 to 0.09375
- key_projector: bfloat16 [4096, 1024], P('kv', ('dp', 'tp')), may hold values from -0.09375 to 0.09375
- value_projector: bfloat16 [4096, 2048], P('kv', ('dp', 'tp')), may hold values from -0.09375 to 0.09375
- output_gate_weight: bfloat16 [4096, 2048], P('kv', ('dp', 'tp')), may hold values from -0.09375 to 0.09375
- forget_weight: bfloat16 [4096, 1024], P('kv', ('dp', 'tp')), may hold values from -0.75 to 0.75
- head_norm_gain: float32 [128], replicated, may hold values from 0.1 to 1.9
- output_projector: bfloat16 [2048, 4096], P(('dp', 'tp'), 'kv'), may hold values from -0.125 to 0.125
- trailing_norm_gain: float32 [4096], P('kv'), may hold values from 0.1 to 1.9
- trailing_gate_weight: bfloat16 [4096, 11264], P('kv', ('dp', 'tp')), may hold values from -0.09375 to 0.09375
- trailing_up_weight: bfloat16 [4096, 11264], P('kv', ('dp', 'tp')), may hold values from -0.09375 to 0.09375
- trailing_down_weight: bfloat16 [11264, 4096], P(('dp', 'tp'), 'kv'), may hold values from -0.0546875 to 0.0546875
Outputs:
- result: bfloat16 [128, 4096], P(('grp', 'dp', 'tp'), 'kv'), parts along dimension 0
- new_state: float32 [128, 16, 64, 128], P(('grp', 'kv'), ('dp', 'tp')), parts along dimension 0
There are 2 independent parts, one for each index of `grp`. A program takes and returns all parts, laid end to end along the dimension named above; an argument that names none is the same for every part. Nothing has to cross between parts.
All inputs are finite; a program needn't handle non-finite values.
Results may differ from a plain program's by a relative error of at most 0.0095.
Values may be sent and summed in bfloat16 or wider, within the bound.
A program may use at most 128 MiB of HBM per device.

v0:
```python
import jax
import jax.numpy as jnp
from jax import lax
from jax.sharding import PartitionSpec as P

D = 4096
KEY_CHANNELS = 64
VALUE_DIM = 128


epsilon = 1e-06


def batch_rows(row_block):
    return lax.all_gather(row_block, ("dp", "tp"), axis=0, tiled=True)


def channel_mixer(row_block, norm_gain, gate_matrix, up_matrix, down_matrix):
    gathered = batch_rows(row_block)
    widened = gathered.astype(jnp.float32)
    squares = jnp.sum(widened * widened, axis=1)
    scaled = (widened * norm_gain).astype(jnp.bfloat16)
    gate_part = jnp.dot(scaled, gate_matrix, preferred_element_type=jnp.float32)
    up_part = jnp.dot(scaled, up_matrix, preferred_element_type=jnp.float32)
    gate_sum, up_sum, row_total = (
        lax.psum_scatter(gate_part, "kv", scatter_dimension=0, tiled=True),
        lax.psum_scatter(up_part, "kv", scatter_dimension=0, tiled=True),
        lax.psum_scatter(squares, "kv", scatter_dimension=0, tiled=True),
    )
    decay_factor = lax.rsqrt(row_total / D + epsilon)[:, None]
    hidden_share = (jax.nn.silu(decay_factor * gate_sum) * (decay_factor * up_sum)).astype(
        jnp.bfloat16
    )
    hidden = lax.all_gather(hidden_share, "kv", axis=0, tiled=True)
    return lax.psum_scatter(
        jnp.dot(hidden, down_matrix, preferred_element_type=jnp.float32),
        ("dp", "tp"),
        scatter_dimension=0,
        tiled=True,
    )


def per_device(
    residual_input,
    incoming_state,
    extra_log_decay,
    leading_norm_gain,
    leading_gate_weight,
    leading_up_weight,
    leading_down_weight,
    attention_norm_gain,
    query_projector,
    key_projector,
    value_projector,
    output_gate_weight,
    forget_weight,
    head_norm_gain,
    output_projector,
    trailing_norm_gain,
    trailing_gate_weight,
    trailing_up_weight,
    trailing_down_weight,
):
    after_first = (
        residual_input.astype(jnp.float32)
        + 0.5
        * channel_mixer(
            residual_input,
            leading_norm_gain,
            leading_gate_weight,
            leading_up_weight,
            leading_down_weight,
        )
    ).astype(jnp.bfloat16)
    gathered = batch_rows(after_first)
    widened = gathered.astype(jnp.float32)
    squares = jnp.sum(widened * widened, axis=1)
    scaled = (widened * attention_norm_gain).astype(jnp.bfloat16)
    query_part = jnp.dot(scaled, query_projector, preferred_element_type=jnp.float32)
    key_part = jnp.dot(scaled, key_projector, preferred_element_type=jnp.float32)
    value_part = jnp.dot(scaled, value_projector, preferred_element_type=jnp.float32)
    gate_part = jnp.dot(scaled, output_gate_weight, preferred_element_type=jnp.float32)
    decay_part = jnp.dot(scaled, forget_weight, preferred_element_type=jnp.float32)
    query_sum, key_sum, value_sum, gate_sum, decay_total, row_total = (
        lax.psum_scatter(query_part, "kv", scatter_dimension=0, tiled=True),
        lax.psum_scatter(key_part, "kv", scatter_dimension=0, tiled=True),
        lax.psum_scatter(value_part, "kv", scatter_dimension=0, tiled=True),
        lax.psum_scatter(gate_part, "kv", scatter_dimension=0, tiled=True),
        lax.psum_scatter(decay_part, "kv", scatter_dimension=0, tiled=True),
        lax.psum_scatter(squares, "kv", scatter_dimension=0, tiled=True),
    )
    decay_factor = lax.rsqrt(row_total / D + epsilon)[:, None]
    row_count = query_sum.shape[0]
    heads_here = query_sum.shape[1] // KEY_CHANNELS
    queries = (decay_factor * query_sum).reshape(
        row_count, heads_here, KEY_CHANNELS
    ) * KEY_CHANNELS ** (-0.5)
    key_rows = (decay_factor * key_sum).reshape(row_count, heads_here, KEY_CHANNELS)
    value_rows = (decay_factor * value_sum).reshape(row_count, heads_here, VALUE_DIM)
    gate_rows = (decay_factor * gate_sum).reshape(row_count, heads_here, VALUE_DIM)
    decay_logarithm = (
        jax.nn.log_sigmoid(decay_factor * decay_total) / 16.0 + extra_log_decay
    ).reshape(row_count, heads_here, KEY_CHANNELS)
    new_state = (
        jnp.exp(decay_logarithm)[..., None] * incoming_state
        + key_rows[..., None] * value_rows[:, :, None, :]
    )
    read_out = jnp.einsum("bhk,bhkv->bhv", queries, new_state, precision=lax.Precision.HIGHEST)
    normed = read_out * lax.rsqrt(jnp.mean(read_out * read_out, axis=-1, keepdims=True) + epsilon)
    head_rows = (
        (normed * head_norm_gain * jax.nn.silu(gate_rows))
        .astype(jnp.bfloat16)
        .reshape(row_count, heads_here * VALUE_DIM)
    )
    all_heads = lax.all_gather(head_rows, "kv", axis=0, tiled=True)
    mixed_rows = lax.psum_scatter(
        jnp.dot(all_heads, output_projector, preferred_element_type=jnp.float32),
        ("dp", "tp"),
        scatter_dimension=0,
        tiled=True,
    )
    second = (after_first.astype(jnp.float32) + mixed_rows).astype(jnp.bfloat16)
    result = (
        second.astype(jnp.float32)
        + 0.5
        * channel_mixer(
            second,
            trailing_norm_gain,
            trailing_gate_weight,
            trailing_up_weight,
            trailing_down_weight,
        )
    ).astype(jnp.bfloat16)
    return (result, new_state)


def solution(mesh):
    return jax.shard_map(
        per_device,
        mesh=mesh,
        in_specs=(
            P(("grp", "dp", "tp"), "kv"),
            P(("grp", "kv"), ("dp", "tp"), None, None),
            P(("grp", "kv"), ("dp", "tp")),
            P("kv"),
            P("kv", ("dp", "tp")),
            P("kv", ("dp", "tp")),
            P(("dp", "tp"), "kv"),
            P("kv"),
            P("kv", ("dp", "tp")),
            P("kv", ("dp", "tp")),
            P("kv", ("dp", "tp")),
            P("kv", ("dp", "tp")),
            P("kv", ("dp", "tp")),
            P(),
            P(("dp", "tp"), "kv"),
            P("kv"),
            P("kv", ("dp", "tp")),
            P("kv", ("dp", "tp")),
            P(("dp", "tp"), "kv"),
        ),
        out_specs=(P(("grp", "dp", "tp"), "kv"), P(("grp", "kv"), ("dp", "tp"), None, None)),
        check_vma=False,
    )
```

profile of v0, /device:TPU:0, one launch (start us, length us, event | category | flops | bytes accessed | tf_op | source)
XLA Modules:
  0.0 359.7 jit_solution(16201497556303995588)
XLA Ops:
  7.2 6.9 %all_gather.18 = bf16[64,1024]{1,0:T(8,128)(2,1)S(1)} all-gather(bf16[16,1024]{1,0:T(8,128)(2,1)} %param.19), channel_id=1, replica_groups=mesh['grp'=2,'dp'=2,'kv'=4,'tp'=2] {'dp','tp'}, dimensions={0}, use_global_device_ids=true | all-gather | bytes 163840 | tf_op jit(solution)/shard_map/all_gather | solution.py:15
  14.1 4.6 %fusion.10 = f32[64,2816]{1,0:T(8,128)} fusion(bf16[1024,2816]{1,0:T(8,128)(2,1)} %param.24, bf16[64,1024]{1,0:T(8,128)(2,1)S(1)} %all_gather.18, f32[1024]{0:T(1024)} %param.22), kind=kOutput, calls=%fused_computation.17 | convolution fusion | flops 369295360 | bytes 6623232 | tf_op jit(solution)/shard_map/dot_general | solution.py:24
  18.8 4.6 %fusion.12 = f32[64,2816]{1,0:T(8,128)} fusion(bf16[1024,2816]{1,0:T(8,128)(2,1)} %param.23, bf16[64,1024]{1,0:T(8,128)(2,1)S(1)} %all_gather.18, f32[1024]{0:T(1024)S(1)} %copy-done.7), kind=kOutput, calls=%fused_computation.18 | convolution fusion | flops 369295360 | bytes 6623232 | tf_op jit(solution)/shard_map/dot_general | solution.py:23
  24.9 12.7 %all-reduce = f32[64]{0:T(128)S(1)} all-reduce(f32[64]{0:T(128)S(1)} %fusion), channel_id=2, replica_groups=mesh['grp'=2,'dp'=2,'kv'=4,'tp'=2] {'kv'}, use_global_device_ids=true, to_apply=%region_1.0.clone | all-reduce | flops 64 | bytes 512
  37.6 6.1 %reduce-scatter.15.cloned.1.call-done = f32[16,2816]{1,0:T(8,128)} async-done(((f32[64,2816]{1,0:T(8,128)}), f32[16,2816]{1,0:T(8,128)}) %reduce-scatter.15.cloned.1.call-update) | async-done | bytes 180240 | tf_op jit(solution)/shard_map/reduce_scatter | solution.py:27
  43.7 24.4 %reduce-scatter.13.cloned.1.call-done = f32[16,2816]{1,0:T(8,128)} async-done(((f32[64,2816]{1,0:T(8,128)}), f32[16,2816]{1,0:T(8,128)}) %reduce-scatter.13.cloned.1.call-update) | async-done | bytes 180240 | tf_op jit(solution)/shard_map/reduce_scatter | solution.py:26
  69.3 15.1 %all_gather.19 = bf16[64,2816]{1,0:T(8,128)(2,1)S(1)} all-gather(bf16[16,2816]{1,0:T(8,128)(2,1)S(1)} %multiply_convert_fusion.1), channel_id=1, replica_groups=mesh['grp'=2,'dp'=2,'kv'=4,'tp'=2] {'kv'}, dimensions={0}, use_global_device_ids=true | all-gather | bytes 450560 | tf_op jit(solution)/shard_map/all_gather | solution.py:34
  88.9 19.0 %reduce-scatter.17.cloned.1.call-done = f32[16,1024]{1,0:T(8,128)} async-done(((f32[64,1024]{1,0:T(8,128)}), f32[16,1024]{1,0:T(8,128)}) %reduce-scatter.17.cloned.1.call-update) | async-done | bytes 65552 | tf_op jit(solution)/shard_map/reduce_scatter | solution.py:35
  108.8 5.4 %all_gather.20 = bf16[64,1024]{1,0:T(8,128)(2,1)S(1)} all-gather(bf16[16,1024]{1,0:T(8,128)(2,1)S(1)} %add_convert_fusion.2), channel_id=1, replica_groups=mesh['grp'=2,'dp'=2,'kv'=4,'tp'=2] {'dp','tp'}, dimensions={0}, use_global_device_ids=true | all-gather | bytes 163840 | tf_op jit(solution)/shard_map/all_gather | solution.py:15
  121.3 11.8 %all-reduce.1 = f32[64]{0:T(128)S(1)} all-reduce(f32[64]{0:T(128)S(1)} %fusion.2), channel_id=6, replica_groups=mesh['grp'=2,'dp'=2,'kv'=4,'tp'=2] {'kv'}, use_global_device_ids=true, to_apply=%region_6.7.clone | all-reduce | flops 64 | bytes 512
  135.6 19.5 %reduce-scatter.23.cloned.1.call-done = f32[16,256]{1,0:T(8,128)} async-done(((f32[64,256]{1,0:T(8,128)}), f32[16,256]{1,0:T(8,128)}) %reduce-scatter.23.cloned.1.call-update) | async-done | bytes 16400 | tf_op jit(solution)/shard_map/reduce_scatter | solution.py:86
  155.2 19.6 %reduce-scatter.19.cloned.1.call-done = f32[16,256]{1,0:T(8,128)} async-done(((f32[64,256]{1,0:T(8,128)}), f32[16,256]{1,0:T(8,128)}) %reduce-scatter.19.cloned.1.call-update) | async-done | bytes 16400 | tf_op jit(solution)/shard_map/reduce_scatter | solution.py:85
  175.9 18.8 %reduce-scatter.27.cloned.1.call-done = f32[16,512]{1,0:T(8,128)} async-done(((f32[64,512]{1,0:T(8,128)}), f32[16,512]{1,0:T(8,128)}) %reduce-scatter.27.cloned.1.call-update) | async-done | bytes 32784 | tf_op jit(solution)/shard_map/reduce_scatter | solution.py:88
  194.7 20.5 %reduce-scatter.25.cloned.1.call-done = f32[16,512]{1,0:T(8,128)} async-done(((f32[64,512]{1,0:T(8,128)}), f32[16,512]{1,0:T(8,128)}) %reduce-scatter.25.cloned.1.call-update) | async-done | bytes 32784 | tf_op jit(solution)/shard_map/reduce_scatter | solution.py:87
  220.6 13.1 %all_gather.21 = bf16[64,512]{1,0:T(8,128)(2,1)S(1)} all-gather(bf16[16,512]{1,0:T(8,128)(2,1)S(1)} %bitcast.28), channel_id=1, replica_groups=mesh['grp'=2,'dp'=2,'kv'=4,'tp'=2] {'kv'}, dimensions={0}, use_global_device_ids=true | all-gather | bytes 81920 | tf_op jit(solution)/shard_map/all_gather | solution.py:115
  234.8 18.3 %reduce-scatter.29.cloned.1.call-done = f32[16,1024]{1,0:T(8,128)} async-done(((f32[64,1024]{1,0:T(8,128)}), f32[16,1024]{1,0:T(8,128)}) %reduce-scatter.29.cloned.1.call-update) | async-done | bytes 65552 | tf_op jit(solution)/shard_map/reduce_scatter | solution.py:116
  254.0 5.4 %all_gather.22 = bf16[64,1024]{1,0:T(8,128)(2,1)S(1)} all-gather(bf16[16,1024]{1,0:T(8,128)(2,1)S(1)} %add_convert_fusion.1), channel_id=1, replica_groups=mesh['grp'=2,'dp'=2,'kv'=4,'tp'=2] {'dp','tp'}, dimensions={0}, use_global_device_ids=true | all-gather | bytes 163840 | tf_op jit(solution)/shard_map/all_gather | solution.py:15
  259.4 4.6 %fusion.6 = f32[64,2816]{1,0:T(8,128)} fusion(bf16[1024,2816]{1,0:T(8,128)(2,1)} %param.36, bf16[64,1024]{1,0:T(8,128)(2,1)S(1)} %all_gather.22, f32[1024]{0:T(1024)S(1)} %copy-done.8), kind=kOutput, calls=%fused_computation.15 | convolution fusion | flops 369295360 | bytes 6623232 | tf_op jit(solution)/shard_map/dot_general | solution.py:24
  264.1 4.6 %fusion.8 = f32[64,2816]{1,0:T(8,128)} fusion(bf16[1024,2816]{1,0:T(8,128)(2,1)} %param.35, bf16[64,1024]{1,0:T(8,128)(2,1)S(1)} %all_gather.22, f32[1024]{0:T(1024)S(1)} %copy-done.8), kind=kOutput, calls=%fused_computation.16 | convolution fusion | flops 369295360 | bytes 6623232 | tf_op jit(solution)/shard_map/dot_general | solution.py:23
  268.9 12.0 %all-reduce.2 = f32[64]{0:T(128)S(1)} all-reduce(f32[64]{0:T(128)S(1)} %fusion.4), channel_id=13, replica_groups=mesh['grp'=2,'dp'=2,'kv'=4,'tp'=2] {'kv'}, use_global_device_ids=true, to_apply=%region_15.16.clone | all-reduce | flops 64 | bytes 512
  281.0 6.4 %reduce-scatter.33.cloned.1.call-done = f32[16,2816]{1,0:T(8,128)} async-done(((f32[64,2816]{1,0:T(8,128)}), f32[16,2816]{1,0:T(8,128)}) %reduce-scatter.33.cloned.1.call-update) | async-done | bytes 180240 | tf_op jit(solution)/shard_map/reduce_scatter | solution.py:27
  287.4 24.3 %reduce-scatter.31.cloned.1.call-done = f32[16,2816]{1,0:T(8,128)} async-done(((f32[64,2816]{1,0:T(8,128)}), f32[16,2816]{1,0:T(8,128)}) %reduce-scatter.31.cloned.1.call-update) | async-done | bytes 180240 | tf_op jit(solution)/shard_map/reduce_scatter | solution.py:26
  312.8 14.9 %all_gather.23 = bf16[64,2816]{1,0:T(8,128)(2,1)S(1)} all-gather(bf16[16,2816]{1,0:T(8,128)(2,1)S(1)} %multiply_convert_fusion), channel_id=1, replica_groups=mesh['grp'=2,'dp'=2,'kv'=4,'tp'=2] {'kv'}, dimensions={0}, use_global_device_ids=true | all-gather | bytes 450560 | tf_op jit(solution)/shard_map/all_gather | solution.py:34
  332.2 19.2 %reduce-scatter.35.cloned.1.call-done = f32[16,1024]{1,0:T(8,128)} async-done(((f32[64,1024]{1,0:T(8,128)}), f32[16,1024]{1,0:T(8,128)}) %reduce-scatter.35.cloned.1.call-update) | async-done | bytes 65552 | tf_op jit(solution)/shard_map/reduce_scatter | solution.py:35
  (80 shorter events, 32.8 us)
Async XLA Ops:
  7.2 226.6 %copy-start = (bf16[512,1024]{1,0:T(8,128)(2,1)S(1)}, bf16[512,1024]{1,0:T(8,128)(2,1)}, u32[]{:S(2)}) copy-start(bf16[512,1024]{1,0:T(8,128)(2,1)} %param.33) | copy-start | bytes 3145732
  7.2 11.6 %copy-start.7 = (f32[1024]{0:T(1024)S(1)}, f32[1024]{0:T(1024)}, u32[]{:S(2)}) copy-start(f32[1024]{0:T(1024)} %param.22) | copy-start | bytes 12292
  7.2 36.5 %reduce-scatter.15.cloned.1.call-start = ((), (), s32[]{:S(2)}) async-start(), calls=%async_computation.13 | async-start | bytes 901120 | tf_op jit(solution)/shard_map/reduce_scatter | solution.py:27
  14.1 9.4 %copy-start.10 = (u32[32]{0:T(128)S(1)}, u32[32]{0:T(128)}, u32[]{:S(2)}) copy-start(u32[32]{0:T(128)} %constant.31) | copy-start | bytes 388
  18.8 49.4 %reduce-scatter.13.cloned.1.call-start = ((), (), s32[]{:S(2)}) async-start(), calls=%async_computation.12 | async-start | bytes 901120 | tf_op jit(solution)/shard_map/reduce_scatter | solution.py:26
  23.4 84.5 %copy-start.4 = (bf16[16,1024]{1,0:T(8,128)(2,1)S(1)}, bf16[16,1024]{1,0:T(8,128)(2,1)}, u32[]{:S(2)}) copy-start(bf16[16,1024]{1,0:T(8,128)(2,1)} %param.19) | copy-start | bytes 98308
  23.4 90.8 %copy-start.5 = (f32[1024]{0:T(1024)S(1)}, f32[1024]{0:T(1024)}, u32[]{:S(2)}) copy-start(f32[1024]{0:T(1024)} %param.26) | copy-start | bytes 12292
  23.4 96.7 %copy-start.2 = (bf16[1024,512]{1,0:T(8,128)(2,1)S(1)}, bf16[1024,512]{1,0:T(8,128)(2,1)}, u32[]{:S(2)}) copy-start(bf16[1024,512]{1,0:T(8,128)(2,1)} %param.30) | copy-start | bytes 3145732
  23.5 84.5 %reduce-scatter.17.cloned.1.call-start = ((), (), s32[]{:S(2)}) async-start(), calls=%async_computation.14 | async-start | bytes 327680 | tf_op jit(solution)/shard_map/reduce_scatter | solution.py:35
  69.3 63.8 %copy-start.3 = (bf16[1024,512]{1,0:T(8,128)(2,1)S(1)}, bf16[1024,512]{1,0:T(8,128)(2,1)}, u32[]{:S(2)}) copy-start(bf16[1024,512]{1,0:T(8,128)(2,1)} %param.29) | copy-start | bytes 3145732
  84.4 90.4 %copy-start.6 = (f32[16,256]{1,0:T(8,128)S(1)}, f32[16,256]{1,0:T(8,128)}, u32[]{:S(2)}) copy-start(f32[16,256]{1,0:T(8,128)} %param.21) | copy-start | bytes 49156
  88.9 46.8 %reduce-scatter.21.cloned.1.call-start = ((), (), s32[]{:S(2)}) async-start(), calls=%async_computation.16 | async-start | bytes 81920 | tf_op jit(solution)/shard_map/reduce_scatter | solution.py:89
  116.2 104.3 %copy-start.9 = (f32[128]{0:T(128)S(1)}, f32[128]{0:T(128)}, u32[]{:S(2)}) copy-start(f32[128]{0:T(128)} %param.32) | copy-start | bytes 1540
  116.2 39.0 %reduce-scatter.23.cloned.1.call-start = ((), (), s32[]{:S(2)}) async-start(), calls=%async_computation.17 | async-start | bytes 81920 | tf_op jit(solution)/shard_map/reduce_scatter | solution.py:86
  118.1 56.6 %reduce-scatter.19.cloned.1.call-start = ((), (), s32[]{:S(2)}) async-start(), calls=%async_computation.15 | async-start | bytes 81920 | tf_op jit(solution)/shard_map/reduce_scatter | solution.py:85
  120.1 74.6 %reduce-scatter.27.cloned.1.call-start = ((), (), s32[]{:S(2)}) async-start(), calls=%async_computation.19 | async-start | bytes 163840 | tf_op jit(solution)/shard_map/reduce_scatter | solution.py:88
  121.1 138.3 %copy-start.8 = (f32[1024]{0:T(1024)S(1)}, f32[1024]{0:T(1024)}, u32[]{:S(2)}) copy-start(f32[1024]{0:T(1024)} %param.34) | copy-start | bytes 12292
  121.1 94.1 %reduce-scatter.25.cloned.1.call-start = ((), (), s32[]{:S(2)}) async-start(), calls=%async_computation.18 | async-start | bytes 163840 | tf_op jit(solution)/shard_map/reduce_scatter | solution.py:87
  134.0 119.1 %reduce-scatter.29.cloned.1.call-start = ((), (), s32[]{:S(2)}) async-start(), calls=%async_computation.20 | async-start | bytes 327680 | tf_op jit(solution)/shard_map/reduce_scatter | solution.py:116
  218.5 45.5 %copy-start.1 = (f32[16,4,64,128]{3,2,1,0:T(8,128)}, f32[16,4,64,128]{3,2,1,0:T(8,128)S(1)}, u32[]{:S(2)}) copy-start(f32[16,4,64,128]{3,2,1,0:T(8,128)S(1)} %multiply_add_fusion) | copy-start | bytes 6291460
  234.7 52.6 %reduce-scatter.33.cloned.1.call-start = ((), (), s32[]{:S(2)}) async-start(), calls=%async_computation.22 | async-start | bytes 901120 | tf_op jit(solution)/shard_map/reduce_scatter | solution.py:27
  264.0 47.6 %reduce-scatter.31.cloned.1.call-start = ((), (), s32[]{:S(2)}) async-start(), calls=%async_computation.21 | async-start | bytes 901120 | tf_op jit(solution)/shard_map/reduce_scatter | solution.py:26
  268.7 82.7 %reduce-scatter.35.cloned.1.call-start = ((), (), s32[]{:S(2)}) async-start(), calls=%async_computation.23 | async-start | bytes 327680 | tf_op jit(solution)/shard_map/reduce_scatter | solution.py:35
Sparse Core Ops, SparseCore 0:
  18.9 24.7 reduce-scatter.14
  46.0 22.0 reduce-scatter.12
  89.0 18.9 reduce-scatter.16
  116.3 19.3 reduce-scatter.20
  137.7 17.4 reduce-scatter.22
  157.3 17.4 reduce-scatter.18
  177.0 17.6 reduce-scatter.26
  197.5 17.6 reduce-scatter.24
  234.9 18.2 reduce-scatter.28
  264.1 23.1 reduce-scatter.32
  289.7 21.9 reduce-scatter.30
  332.3 18.9 reduce-scatter.34
where the time goes:
time: 361 us; the launch traced here: 360 us
  waiting for transfers between devices  198 us (55%)
  blocking collectives  97.3 us (27%)
  matrix products  37.8 us (10%)
  between operations  15 us (4%)
  other arithmetic  10.4 us (3%)
    reduce_scatter x2, waiting for transfers between devices, channel_mixer(): lax.psum_scatter(gate_part, 'kv', scatter_dimension=0, tiled=True)  48.7 us
    reduce_scatter x2, waiting for transfers between devices, channel_mixer(): lax.psum_scatter(jnp.dot(hidden, down_matrix, preferred_element_type=jnp....  38.2 us
    unnamed x3, blocking collectives  36.4 us
    all_gather x2, blocking collectives, channel_mixer(): hidden = lax.all_gather(hidden_share, 'kv', axis=0, tiled=True)  30 us
    reduce_scatter x1, waiting for transfers between devices, per_device(): lax.psum_scatter(value_part, 'kv', scatter_dimension=0, tiled=True)  20.5 us
    reduce_scatter x1, waiting for transfers between devices, per_device(): lax.psum_scatter(query_part, 'kv', scatter_dimension=0, tiled=True)  19.6 us
    reduce_scatter x1, waiting for transfers between devices, per_device(): lax.psum_scatter(key_part, 'kv', scatter_dimension=0, tiled=True)  19.5 us
    reduce_scatter x1, waiting for transfers between devices, per_device(): lax.psum_scatter(gate_part, 'kv', scatter_dimension=0, tiled=True)  18.8 us
  transfers between devices with their start and end apart: 12, of which 12 were waited for; matrix products, arithmetic and copies ran while one was open for 5% of the time, Pallas kernels for 0%

commit v1 on v0

v1 whole, which is shorter than its diff:
```python
import functools

import jax
import jax.numpy as jnp
from jax import lax
from jax.experimental import pallas as pl
from jax.experimental.pallas import tpu as pltpu
from jax.sharding import PartitionSpec as P

KEY_CHANNELS = 64
VALUE_DIM = 128
LANES = 128
epsilon = 1e-06
MESH = pl.DeviceIdType.MESH
F32 = jnp.float32
BF16 = jnp.bfloat16
CHUNKS = 4


def spans(width, count):
    if width % LANES:
        return [(0, width)]
    tile = 2 * LANES if width % (2 * LANES) == 0 else LANES
    tiles = width // tile
    count = min(count, tiles)
    cuts = [tile * ((tiles * i + count - 1) // count) for i in range(count + 1)]
    return list(zip(cuts[:-1], cuts[1:]))


def padded(width):
    return -(-width // LANES) * LANES


def silu(x):
    return x * jax.nn.sigmoid(x)


def kernel(dims, names, *refs):
    R, K, TP, D, B, d, F, W, V, heads = dims
    mr, mk = B // R, B // K
    ref = dict(zip(names, refs))
    dp_i, tp_i, k = lax.axis_index("dp"), lax.axis_index("tp"), lax.axis_index("kv")
    r = dp_i * TP + tp_i
    Wp = padded(W)
    kv_order = sorted(range(1, K), key=lambda o: abs(2 * o - K))
    counter = {"send": 0, "local": 0}
    pending = []

    def row_peer(o):
        t = lax.rem(r + o, R)
        return t, {"dp": t // TP, "tp": lax.rem(t, TP)}

    def kv_peer(o):
        t = lax.rem(k + o, K)
        return t, {"kv": t}

    def local(src, dst):
        i = counter["local"]
        counter["local"] += 1
        copy = pltpu.make_async_copy(src, dst, ref["local_sem"].at[i])
        copy.start()
        return copy

    def remote(src, dst, device):
        i = counter["send"]
        counter["send"] += 1
        copy = pltpu.make_async_remote_copy(
            src_ref=src,
            dst_ref=dst,
            send_sem=ref["send_sem"].at[i],
            recv_sem=ref["recv_sem"].at[i],
            device_id=device,
            device_id_type=MESH,
        )
        copy.start()
        pending.append(copy)
        return copy

    own_x = local(ref["x"], ref["x_all"].at[r])
    load_g1 = local(ref["g1"], ref["g1_v"])
    fspans = spans(F, CHUNKS)

    def load_mixer(p):
        first = []
        for a, b in fspans:
            cut = (slice(None), slice(None)) if b - a == F else (slice(None), pl.ds(a, b - a))
            first.append(
                (
                    local(ref[p + "g"].at[cut], ref[p + "g_v"].at[cut]),
                    local(ref[p + "u"].at[cut], ref[p + "u_v"].at[cut]),
                )
            )
        return first, local(ref[p + "d"], ref[p + "d_v"])

    lead = load_mixer("l")
    load_attn = [local(ref[n], ref[n + "_v"]) for n in ("g2", "wq", "wk", "wf", "wv", "wg")]
    load_state = [local(ref[n], ref[n + "_v"]) for n in ("st", "eld", "hng")]
    load_out = local(ref["wo"], ref["wo_v"])
    load_g3 = local(ref["g3"], ref["g3_v"])
    trail = load_mixer("t")

    barrier = pltpu.get_barrier_semaphore()
    for o in range(1, R):
        pl.semaphore_signal(barrier, inc=1, device_id=row_peer(o)[1], device_id_type=MESH)
    for o in kv_order:
        pl.semaphore_signal(barrier, inc=1, device_id=kv_peer(o)[1], device_id_type=MESH)
    pl.semaphore_wait(barrier, R - 1 + K - 1)

    def gather_rows(src, buf):
        copies = [remote(src, buf.at[r], row_peer(o)[1]) for o in range(1, R)]
        return copies

    def wait_all(copies):
        for copy in copies:
            copy.wait_recv()

    def normalised(buf, gain):
        wide = buf[...].reshape(B, d).astype(F32)
        squares = jnp.sum(wide * wide, axis=1, keepdims=True)
        ref["scaled"][...] = (wide * gain[...]).astype(BF16)
        return jnp.broadcast_to(squares, (B, LANES)).reshape(K, mk, LANES)

    def row_scale(total):
        return lax.rsqrt(total / D + epsilon)[:, :1]

    def mixer(p, buf, gain, loads):
        gu_loads, down_load = loads
        gu_send, gu_recv = ref[p + "gu_send"], ref[p + "gu_recv"]
        ss_send, ss_recv = ref[p + "ss_send"], ref[p + "ss_recv"]
        h_all = ref[p + "h_all"]
        ss_send[...] = normalised(buf, gain)
        ss_copies = []
        for o in kv_order:
            t, device = kv_peer(o)
            ss_copies.append(remote(ss_send.at[t], ss_recv.at[o - 1], device))
        gu_copies = []
        for (a, b), pair in zip(fspans, gu_loads):
            for i, part in enumerate("gu"):
                pair[i].wait()
                product = jnp.dot(
                    ref["scaled"][...], ref[p + part + "_v"][:, a:b], preferred_element_type=F32
                )
                gu_send[:, i, :, a:b] = product.astype(BF16).reshape(K, mk, b - a)
            group = []
            for o in kv_order:
                t, device = kv_peer(o)
                if b - a == F:
                    src, dst = gu_send.at[t], gu_recv.at[o - 1]
                else:
                    src = gu_send.at[t, :, :, pl.ds(a, b - a)]
                    dst = gu_recv.at[o - 1, :, :, pl.ds(a, b - a)]
                group.append(remote(src, dst, device))
            gu_copies.append(group)
        wait_all(ss_copies)
        total = ss_send[k]
        for o in kv_order:
            total = total + ss_recv[o - 1]
        scale = row_scale(total)
        h_copies = []
        for (a, b), group in zip(fspans, gu_copies):
            wait_all(group)
            gate = gu_send[k, 0, :, a:b].astype(F32)
            up = gu_send[k, 1, :, a:b].astype(F32)
            for o in kv_order:
                gate = gate + gu_recv[o - 1, 0, :, a:b].astype(F32)
                up = up + gu_recv[o - 1, 1, :, a:b].astype(F32)
            h_all[k, :, a:b] = (silu(scale * gate) * (scale * up)).astype(BF16)
            mine = h_all.at[k] if b - a == F else h_all.at[k, :, pl.ds(a, b - a)]
            h_copies.append([remote(mine, mine, kv_peer(o)[1]) for o in kv_order])
        down_load.wait()
        acc = None
        for (a, b), group in zip(fspans, h_copies):
            wait_all(group)
            part = jnp.dot(
                h_all[:, :, a:b].reshape(B, b - a),
                ref[p + "d_v"][a:b, :],
                preferred_element_type=F32,
            )
            acc = part if acc is None else acc + part
        return acc

    def scatter_rows(p, value):
        send, recv = ref[p + "_send"], ref[p + "_recv"]
        send[...] = value.astype(BF16).reshape(R, mr, d)
        copies = []
        for o in range(1, R):
            t, device = row_peer(o)
            copies.append(remote(send.at[t], recv.at[o - 1], device))
        wait_all(copies)
        total = send[r].astype(F32)
        for o in range(1, R):
            total = total + recv[o - 1].astype(F32)
        return total

    x_copies = gather_rows(ref["x"], ref["x_all"])
    own_x.wait()
    load_g1.wait()
    wait_all(x_copies)
    share = scatter_rows("p1", mixer("l", ref["x_all"], ref["g1_v"], lead))
    after = (ref["x_all"][r].astype(F32) + 0.5 * share).astype(BF16)
    ref["a_all"][r] = after
    a_copies = gather_rows(ref["a_all"].at[r], ref["a_all"])
    for copy in load_attn:
        copy.wait()
    wait_all(a_copies)

    squares = normalised(ref["a_all"], ref["g2_v"])
    f_send, f_recv = ref["f_send"], ref["f_recv"]
    q_send, q_recv = ref["q_send"], ref["q_recv"]
    v_send, v_recv = ref["v_send"], ref["v_recv"]

    def project(name):
        return jnp.dot(ref["scaled"][...], ref[name + "_v"][...], preferred_element_type=F32)

    f_send[:, :, Wp:] = squares
    f_send[:, :, :W] = project("wf").reshape(K, mk, W)
    f_copies, q_copies, v_copies = [], [], []
    for o in kv_order:
        t, device = kv_peer(o)
        f_copies.append(remote(f_send.at[t], f_recv.at[o - 1], device))
    q_send[:, 0, :, :W] = project("wq").astype(BF16).reshape(K, mk, W)
    q_send[:, 1, :, :W] = project("wk").astype(BF16).reshape(K, mk, W)
    for o in kv_order:
        t, device = kv_peer(o)
        q_copies.append(remote(q_send.at[t], q_recv.at[o - 1], device))
    v_send[:, 0] = project("wv").astype(BF16).reshape(K, mk, V)
    v_send[:, 1] = project("wg").astype(BF16).reshape(K, mk, V)
    for o in kv_order:
        t, device = kv_peer(o)
        v_copies.append(remote(v_send.at[t], v_recv.at[o - 1], device))
    for copy in load_state:
        copy.wait()
    wait_all(f_copies)
    forget = f_send[k]
    for o in kv_order:
        forget = forget + f_recv[o - 1]
    scale = row_scale(forget[:, Wp:])
    forget = scale * forget[:, :W]
    decay = jnp.exp(
        (jnp.minimum(forget, 0.0) - jnp.log1p(jnp.exp(-jnp.abs(forget)))) / 16.0 + ref["eld_v"][...]
    )
    columns = ref["columns"]
    columns[0] = decay.T
    wait_all(q_copies)
    pair = []
    for i in range(2):
        total = q_send[k, i, :, :W].astype(F32)
        for o in kv_order:
            total = total + q_recv[o - 1, i, :, :W].astype(F32)
        pair.append(scale * total)
    columns[1] = pair[1].T
    columns[2] = (pair[0] * KEY_CHANNELS ** (-0.5)).T
    wait_all(v_copies)
    pair = []
    for i in range(2):
        total = v_send[k, i].astype(F32)
        for o in kv_order:
            total = total + v_recv[o - 1, i].astype(F32)
        pair.append(scale * total)
    ref["vals"][...] = pair[0]
    gates = silu(pair[1])
    for b in range(mk):
        for h in range(heads):
            rows = slice(h * KEY_CHANNELS, (h + 1) * KEY_CHANNELS)
            lanes = slice(h * VALUE_DIM, (h + 1) * VALUE_DIM)
            new = (
                columns[0, rows, b : b + 1] * ref["st_v"][b, h]
                + columns[1, rows, b : b + 1] * ref["vals"][b : b + 1, lanes]
            )
            ref["ns_v"][b, h] = new
            ref["read"][b : b + 1, lanes] = jnp.sum(
                columns[2, rows, b : b + 1] * new, axis=0, keepdims=True
            )
    store_state = local(ref["ns_v"], ref["new_state"])
    hr_all = ref["hr_all"]
    for h in range(heads):
        lanes = slice(h * VALUE_DIM, (h + 1) * VALUE_DIM)
        out = ref["read"][:, lanes]
        out = out * lax.rsqrt(jnp.mean(out * out, axis=1, keepdims=True) + epsilon)
        hr_all[k, :, lanes] = (out * ref["hng_v"][...] * gates[:, lanes]).astype(BF16)
    hr_copies = [remote(hr_all.at[k], hr_all.at[k], kv_peer(o)[1]) for o in kv_order]
    load_out.wait()
    wait_all(hr_copies)
    mixed = scatter_rows(
        "p2",
        jnp.dot(hr_all[...].reshape(B, V), ref["wo_v"][...], preferred_element_type=F32),
    )
    second = (ref["a_all"][r].astype(F32) + mixed).astype(BF16)
    ref["s_all"][r] = second
    s_copies = gather_rows(ref["s_all"].at[r], ref["s_all"])
    load_g3.wait()
    wait_all(s_copies)

    share = scatter_rows("p3", mixer("t", ref["s_all"], ref["g3_v"], trail))
    ref["res_v"][...] = (ref["s_all"][r].astype(F32) + 0.5 * share).astype(BF16)
    store_result = local(ref["res_v"], ref["result"])
    for copy in pending:
        copy.wait_send()
    store_state.wait()
    store_result.wait()


ARGS = ("x", "st", "eld", "g1", "lg", "lu", "ld", "g2", "wq", "wk")
ARGS += ("wv", "wg", "wf", "hng", "wo", "g3", "tg", "tu", "td")


def per_device(sizes, *arrays):
    dp, tp, K = sizes
    R = dp * tp
    ref = dict(zip(ARGS, arrays))
    for n in ("g1", "g2", "g3", "hng"):
        ref[n] = ref[n].reshape(1, -1)
    mr, d = ref["x"].shape
    B, D = mr * R, d * K
    mk = B // K
    F = ref["lg"].shape[1]
    W, V = ref["wq"].shape[1], ref["wv"].shape[1]
    heads = W // KEY_CHANNELS
    Wp = padded(W)
    dims = (R, K, tp, D, B, d, F, W, V, heads)
    vm = {}
    for n in ARGS:
        if n != "x":
            vm[n + "_v"] = (ref[n].shape, ref[n].dtype)
    for n in ("x_all", "a_all", "s_all"):
        vm[n] = ((R, mr, d), BF16)
    vm["scaled"] = ((B, d), BF16)
    for p in ("l", "t"):
        vm[p + "gu_send"] = ((K, 2, mk, F), BF16)
        vm[p + "gu_recv"] = ((K - 1, 2, mk, F), BF16)
        vm[p + "ss_send"] = ((K, mk, LANES), F32)
        vm[p + "ss_recv"] = ((K - 1, mk, LANES), F32)
        vm[p + "h_all"] = ((K, mk, F), BF16)
    for p in ("p1", "p2", "p3"):
        vm[p + "_send"] = ((R, mr, d), BF16)
        vm[p + "_recv"] = ((R - 1, mr, d), BF16)
    vm["f_send"] = ((K, mk, Wp + LANES), F32)
    vm["f_recv"] = ((K - 1, mk, Wp + LANES), F32)
    vm["q_send"] = ((K, 2, mk, Wp), BF16)
    vm["q_recv"] = ((K - 1, 2, mk, Wp), BF16)
    vm["v_send"] = ((K, 2, mk, V), BF16)
    vm["v_recv"] = ((K - 1, 2, mk, V), BF16)
    vm["columns"] = ((3, W, mk), F32)
    vm["vals"] = ((mk, V), F32)
    vm["read"] = ((mk, V), F32)
    vm["ns_v"] = (ref["st"].shape, F32)
    vm["hr_all"] = ((K, mk, V), BF16)
    vm["res_v"] = ((mr, d), BF16)
    names = [*ARGS, "result", "new_state", *vm, "local_sem", "send_sem", "recv_sem"]
    sems = 3 * 2 * R + 2 * K * (1 + 2 * CHUNKS) + 4 * K
    return pl.pallas_call(
        functools.partial(kernel, dims, names),
        out_shape=(
            jax.ShapeDtypeStruct((mr, d), BF16),
            jax.ShapeDtypeStruct(ref["st"].shape, F32),
        ),
        in_specs=[pl.BlockSpec(memory_space=pl.ANY)] * len(ARGS),
        out_specs=[pl.BlockSpec(memory_space=pl.ANY)] * 2,
        scratch_shapes=[
            *[pltpu.VMEM(shape, dtype) for shape, dtype in vm.values()],
            pltpu.SemaphoreType.DMA((20 + 6 * CHUNKS,)),
            pltpu.SemaphoreType.DMA((sems,)),
            pltpu.SemaphoreType.DMA((sems,)),
        ],
        compiler_params=pltpu.CompilerParams(
            collective_id=0, has_side_effects=True, vmem_limit_bytes=63 * 1024 * 1024
        ),
    )(*[ref[n] for n in ARGS])


def solution(mesh):
    sizes = (mesh.shape["dp"], mesh.shape["tp"], mesh.shape["kv"])
    return jax.shard_map(
        functools.partial(per_device, sizes),
        mesh=mesh,
        in_specs=(
            P(("grp", "dp", "tp"), "kv"),
            P(("grp", "kv"), ("dp", "tp"), None, None),
            P(("grp", "kv"), ("dp", "tp")),
            P("kv"),
            P("kv", ("dp", "tp")),
            P("kv", ("dp", "tp")),
            P(("dp", "tp"), "kv"),
            P("kv"),
            P("kv", ("dp", "tp")),
            P("kv", ("dp", "tp")),
            P("kv", ("dp", "tp")),
            P("kv", ("dp", "tp")),
            P("kv", ("dp", "tp")),
            P(),
            P(("dp", "tp"), "kv"),
            P("kv"),
            P("kv", ("dp", "tp")),
            P("kv", ("dp", "tp")),
            P(("dp", "tp"), "kv"),
        ),
        out_specs=(P(("grp", "dp", "tp"), "kv"), P(("grp", "kv"), ("dp", "tp"), None, None)),
        check_vma=False,
    )
```

time: 361 us -> 99.3 us (0.28)
  waiting for transfers between devices: 198 us -> 0 us
  blocking collectives: 97.3 us -> 0 us
  Pallas kernels: 0 us -> 93.9 us
  matrix products: 37.8 us -> 0 us
  between operations: 15 us -> 0.65 us
  other arithmetic: 10.4 us -> 0 us
  local copies, waits for them, and re-layouts: 0.92 us -> 4.53 us
    reduce_scatter x12 -> x0, waiting for transfers between devices: 198 us -> none  [the longest x2 48.7 us: channel_mixer(): lax.psum_scatter(gate_part, 'kv', scatter_dimension=0, tiled=True)]
    pallas_call x0 -> x1, Pallas kernels: none -> 93.9 us  [per_device(): pl.pallas_call(functools.partial(kernel, dims, names), out_shape=(jax.Sha...]
    all_gather x6 -> x0, blocking collectives: 60.9 us -> none  [the longest x2 30 us: channel_mixer(): hidden = lax.all_gather(hidden_share, 'kv', axis=0, tiled=True)]
    dot_general x13 -> x0, matrix products: 37.8 us -> none  [the longest x2 9.25 us: channel_mixer(): up_part = jnp.dot(scaled, up_matrix, preferred_element_type=jnp.float32)]
    unnamed x3 -> x0, blocking collectives: 36.4 us -> none
    convert_element_type x6 -> x0, other arithmetic: 5.52 us -> none  [the longest x2 2.27 us: channel_mixer(): (jax.nn.silu(decay_factor * gate_sum) * (decay_factor * up_sum)).astype(j...]
    unnamed x24 -> x2, local copies, waits for them, and re-layouts: 0.65 us -> 4.53 us
  transfers between devices with their start and end apart: 12 -> 0, of which waited for: 12 -> 0; matrix products, arithmetic and copies ran while one was open for 5% -> 0% of each run, Pallas kernels for 0% -> 0%
where the time goes in v1:
time: 99.3 us; the launch traced here: 99.1 us
  Pallas kernels  93.9 us (95%)
  local copies, waits for them, and re-layouts  4.53 us (5%)
    pallas_call x1, Pallas kernels, per_device(): pl.pallas_call(functools.partial(kernel, dims, names), out_shape=(jax.Sha...  93.9 us
    unnamed x2, local copies, waits for them, and re-layouts  4.53 us

profile of v1, /device:TPU:0, one launch (start us, length us, event | category | flops | bytes accessed | tf_op | source)
XLA Modules:
  0.0 99.1 jit_solution(3009337159403054013)
XLA Ops:
  0.6 93.9 %shard_map.194 = (bf16[16,1024]{1,0:T(8,128)(2,1)}, f32[16,4,64,128]{3,2,1,0:T(8,128)}) custom-call(bf16[16,1024]{1,0:T(8,128)(2,1)} %refs_0_.1, f32[16,4,64,128]{3,2,1,0:T(8,128)} %refs_1_.1, f32[16,256]{1,0:T(8,128)} %refs_2_.1, f32[1,1024]{1,0:T(1,128)} %bitcast.4, bf16[1024,2816]{1,0:T(8,128)(2,1)} %refs_4_.1, bf16[1024,2816]{1,0:T(8,128)(2,1)} %refs_5_.1, ...), custom_call_target="tpu_custom_call" | custom-call | tf_op jit(solution)/shard_map/pallas_call | solution.py:351
  94.6 1.4 %copy.23 = bf16[16,1024]{1,0:T(8,128)(2,1)} copy(bf16[16,1024]{1,0:T(8,128)(2,1)} %get-tuple-element.4) | data formatting | bytes 65536
  96.0 3.2 %copy.24 = f32[16,4,64,128]{3,2,1,0:T(8,128)} copy(f32[16,4,64,128]{3,2,1,0:T(8,128)} %get-tuple-element.5) | data formatting | bytes 4194304
